TPU v7x, 32 devices: a whole 2x2x4 slice. The times are simulated.
32 devices in a mesh: ep: 8 (over z, y), tp: 4 (over x, core).
Axes of the slice: x: 2, y: 2, z: 4, core: 2. Of those that a mesh axis runs over, the one named last changes fastest.
Arguments:
- gate_outer: bfloat16 [16384, 1024], P(('ep', 'tp')), may hold values from -6 to 6
- gate_inner: bfloat16 [16384, 1024], P(('ep', 'tp')), may hold values from -6 to 6
- conv_input: bfloat16 [16384, 1024], P(('ep', 'tp')), may hold values from -6 to 6
- conv_taps: float32 [3, 1024], replicated, may hold values from -3.5 to 3.5
- mixer_out_weight: bfloat16 [1024, 2048], replicated, may hold values from -0.1875 to 0.1875
- moe_tokens: bfloat16 [4096, 2048], P(('ep', 'tp')), may hold values from -40 to 40
- norm_gain: float32 [2048], replicated, may hold values from 0.1 to 1.9
- expert_ids: int32 [4096, 4], P(('ep', 'tp')), may hold values from 0 to 31, all different within a row; in each aligned block of 128 rows (0 to 127, 128 to 255, ...) at most 24 rows name the same one
- route_weight: float32 [4096, 4], P(('ep', 'tp')), may hold values from 0.2 to 1
- expert_gate: bfloat16 [32, 2048, 1024], P(('ep', 'tp')), may hold values from -0.39648438 to 0.39648438
- expert_up: bfloat16 [32, 2048, 1024], P(('ep', 'tp')), may hold values from -0.39648438 to 0.39648438
- expert_down: bfloat16 [32, 1024, 2048], P(('ep', 'tp')), may hold values from -0.03125 to 0.03125
Outputs:
- mixed_out: bfloat16 [16384, 2048], P(('ep', 'tp'))
- moe_out: bfloat16 [4096, 2048], P(('ep', 'tp'))
Inputs may be any that keep to these rules, and one draw needn't show every extreme that they name: `expert_ids`: each token names 4 different experts. Among the tokens of one device no expert is named by more than 24 of them, and on some device an expert is named by exactly 24.
All inputs are finite; a program needn't handle non-finite values.
Results may differ from a plain program's by a relative error of at most 0.007.
Values may be sent and summed in bfloat16 or wider, within the bound.
No kernel may reach another device: no remote copies, remote signals or barrier semaphores. Data moves between devices by JAX's collectives and lax.ppermute only.
A program may use at most 128 MiB of HBM per device.

v0:
```python
import jax
import jax.numpy as jnp
from jax import lax
from jax.sharding import PartitionSpec as P

epsilon = 1e-06
clamp_limit = 7.0
alpha_gate = 1.702


def from_behind(value, axis, by):
    length = lax.axis_size(axis)
    pairs = [(i, i + by) for i in range(length) if 0 <= i + by < length]
    return lax.ppermute(value, axis, pairs)


def expert_rows(row_block, gate_weight, up_weight, down_weight):
    gate_pre = jnp.dot(row_block, gate_weight, preferred_element_type=jnp.float32)
    up_pre = jnp.dot(row_block, up_weight, preferred_element_type=jnp.float32)
    gate_pre = jnp.minimum(gate_pre, clamp_limit)
    up_pre = jnp.clip(up_pre, -clamp_limit, clamp_limit)
    hidden = ((up_pre + 1.0) * (gate_pre * jax.nn.sigmoid(alpha_gate * gate_pre))).astype(
        jnp.bfloat16
    )
    return jnp.dot(hidden, down_weight, preferred_element_type=jnp.float32).astype(jnp.bfloat16)


def shards(
    gate_outer,
    gate_inner,
    conv_input,
    conv_taps,
    mixer_out_weight,
    moe_tokens,
    norm_gain,
    expert_ids,
    route_weight,
    expert_gate,
    expert_up,
    expert_down,
):
    reach_rows = conv_taps.shape[0] - 1
    rows_here = gate_inner.shape[0]
    product = (gate_inner.astype(jnp.float32) * conv_input.astype(jnp.float32)).astype(jnp.bfloat16)
    previous = from_behind(product[rows_here - reach_rows :], ("ep", "tp"), 1)
    extended = jnp.concatenate([previous, product], 0).astype(jnp.float32)
    convolved = jnp.zeros(product.shape, jnp.float32)
    for offset in range(conv_taps.shape[0]):
        convolved = convolved + conv_taps[offset][None, :] * extended[offset : offset + rows_here]
    gated_rows = (gate_outer.astype(jnp.float32) * convolved).astype(jnp.bfloat16)
    mixed_out = jnp.dot(gated_rows, mixer_out_weight, preferred_element_type=jnp.float32).astype(
        jnp.bfloat16
    )
    tokens_here = moe_tokens.shape[0]
    width = moe_tokens.shape[1]
    top_count = expert_ids.shape[1]
    experts_all = lax.axis_size("ep") * lax.axis_size("tp")
    capacity = 3 * tokens_here * top_count // (2 * experts_all)
    widened = moe_tokens.astype(jnp.float32)
    normed = (
        widened
        * lax.rsqrt(jnp.mean(widened * widened, axis=-1, keepdims=True) + epsilon)
        * norm_gain[None, :]
    ).astype(jnp.bfloat16)
    mix_weight = route_weight / jnp.sum(route_weight, axis=-1, keepdims=True)
    flat_ids = expert_ids.reshape(-1)
    one_hot = (flat_ids[:, None] == jnp.arange(experts_all, dtype=jnp.int32)[None, :]).astype(
        jnp.int32
    )
    earlier = jnp.cumsum(one_hot, axis=0) - one_hot
    slot_rank = jnp.sum(earlier * one_hot, axis=1)
    slot_index = (flat_ids * capacity + slot_rank).reshape(tokens_here, top_count)
    slot_range = jnp.arange(experts_all * capacity, dtype=jnp.int32)
    dispatch = jnp.any(slot_index[None, :, :] == slot_range[:, None, None], axis=2).astype(
        jnp.bfloat16
    )
    send_rows = jnp.dot(dispatch, normed, preferred_element_type=jnp.float32).astype(jnp.bfloat16)
    send_rows = send_rows.reshape(experts_all, capacity, width)
    received = lax.all_to_all(send_rows, ("ep", "tp"), split_axis=0, concat_axis=0, tiled=True)
    row_block = received.reshape(-1, width)
    expert_out = expert_rows(row_block, expert_gate[0], expert_up[0], expert_down[0])
    returned = lax.all_to_all(
        expert_out.reshape(received.shape), ("ep", "tp"), split_axis=0, concat_axis=0, tiled=True
    )
    flat_rows = returned.reshape(experts_all * capacity, width)
    picked = (
        flat_rows[slot_index.reshape(-1)].astype(jnp.float32).reshape(tokens_here, top_count, width)
    )
    moe_out = jnp.sum(picked * mix_weight[:, :, None], axis=1).astype(jnp.bfloat16)
    return (mixed_out, moe_out)


def solution(mesh):
    in_specs = (
        P(("ep", "tp"), None),
        P(("ep", "tp"), None),
        P(("ep", "tp"), None),
        P(),
        P(),
        P(("ep", "tp"), None),
        P(),
        P(("ep", "tp"), None),
        P(("ep", "tp"), None),
        P(("ep", "tp"), None, None),
        P(("ep", "tp"), None, None),
        P(("ep", "tp"), None, None),
    )
    out_specs = (P(("ep", "tp"), None), P(("ep", "tp"), None))
    return jax.shard_map(shards, mesh=mesh, in_specs=in_specs, out_specs=out_specs, check_vma=False)
```

profile of v0, /device:TPU:16, one launch (start us, length us, event | category | flops | bytes accessed | tf_op | source)
XLA Modules:
  0.0 193.2 jit_solution(18042692835083974034)
XLA Ops:
  0.6 0.8 copy.21
  1.5 0.1 eq.38
  1.6 1.2 reduce-window.6
  2.8 0.2 slice_reduce_fusion
  3.1 0.1 fusion.28
  3.2 0.1 reduce_sum.41
  3.4 0.2 fusion.15
  3.6 1.2 fusion.16
  4.9 2.1 %convolution_convert_fusion = bf16[768,2048]{1,0:T(8,128)(2,1)S(1)} fusion(pred[768,128]{1,0:T(8,128)(4,1)S(1)} %fusion.15, bf16[128,2048]{1,0:T(8,128)(2,1)} %param.17, f32[2048]{0:T(1024)} %param.18, f32[128]{0:T(128)S(1)} %add_rsqrt_fusion), kind=kOutput, calls=%fused_computation.9 | convolution fusion | flops 405274624 | bytes 3777024 | tf_op jit(solution)/shard_map/dot_general | solution.py:77
  7.0 74.9 %all_to_all.10 = bf16[32,24,2048]{2,1,0:T(8,128)(2,1)S(1)} all-to-all(bf16[32,24,2048]{2,1,0:T(8,128)(2,1)S(1)} %bitcast.47), channel_id=1, replica_groups=mesh['ep'=8,'tp'=4] {'ep','tp'}, dimensions={0} | all-to-all | bytes 6291456 | tf_op jit(solution)/shard_map/all_to_all | solution.py:79
  81.9 3.4 %fusion.2 = f32[768,1024]{1,0:T(8,128)S(1)} fusion(bf16[768,2048]{1,0:T(8,128)(2,1)S(1)} %bitcast.49, bf16[1,2048,1024]{2,1,0:T(8,128)(2,1)S(1)} %copy-done.3), kind=kOutput, calls=%fused_computation.3 | convolution fusion | flops 3221225472 | bytes 10485760 | tf_op jit(solution)/shard_map/dot_general | solution.py:18
  85.3 4.0 %multiply_convert_fusion = bf16[768,1024]{1,0:T(8,128)(2,1)S(1)} fusion(f32[768,1024]{1,0:T(8,128)S(1)} %fusion.2, bf16[768,2048]{1,0:T(8,128)(2,1)S(1)} %bitcast.50, bf16[1,2048,1024]{2,1,0:T(8,128)(2,1)S(1)} %copy-done.4), kind=kOutput, calls=%fused_computation.10 | convolution fusion | flops 3229089792 | bytes 12058624 | tf_op jit(solution)/shard_map/dot_general | solution.py:19
  89.4 4.8 %fusion.6 = bf16[768,2048]{1,0:T(8,128)(2,1)} fusion(bf16[768,1024]{1,0:T(8,128)(2,1)S(1)} %multiply_convert_fusion, bf16[1,1024,2048]{2,1,0:T(8,128)(2,1)S(1)} %copy-done.5), kind=kOutput, calls=%fused_computation.8 | convolution fusion | flops 3222798336 | bytes 8912896 | tf_op jit(solution)/shard_map/dot_general | solution.py:25
  94.2 5.6 %all-to-all-start.1 = ((bf16[32,24,2048]{2,1,0:T(8,128)(2,1)}), bf16[32,24,2048]{2,1,0:T(8,128)(2,1)S(1)}, u32[]{:S(2)}, u32[]{:S(2)}) async-start(bf16[32,24,2048]{2,1,0:T(8,128)(2,1)} %bitcast.48), calls=%async_computation.1 | async-start | bytes 6291456 | tf_op jit(solution)/shard_map/all_to_all | solution.py:82
  99.8 1.9 %multiply_convert_fusion.1 = bf16[512,1024]{1,0:T(8,128)(2,1)S(1)} fusion(bf16[512,1024]{1,0:T(8,128)(2,1)} %param.14, bf16[512,1024]{1,0:T(8,128)(2,1)} %param.13), kind=kLoop, calls=%fused_computation.19 | loop fusion | flops 2097152 | bytes 3145728 | tf_op jit(solution)/shard_map/convert_element_type | solution.py:44
  101.8 1.0 copy-done
  102.8 2.2 %collective-permute-start = (bf16[2,1024]{1,0:T(2,128)(2,1)S(1)}, bf16[2,1024]{1,0:T(2,128)(2,1)S(1)}, u32[]{:S(2)}, u32[]{:S(2)}) collective-permute-start(bf16[2,1024]{1,0:T(2,128)(2,1)S(1)} %slice.38), channel_id=1, source_target_pairs={{0,1},{1,2},{2,3},{3,4},{4,5},{5,6},{6,7},{7,8},{8,9},{9,10},{10,1... | collective-permute-start | bytes 12296 | tf_op jit(solution)/shard_map/ppermute | solution.py:14
  105.2 0.1 copy.26
  105.3 66.0 %collective-permute-done = bf16[2,1024]{1,0:T(2,128)(2,1)S(1)} collective-permute-done((bf16[2,1024]{1,0:T(2,128)(2,1)S(1)}, bf16[2,1024]{1,0:T(2,128)(2,1)S(1)}, u32[]{:S(2)}, u32[]{:S(2)}) %collective-permute-start) | collective-permute-done | bytes 4128 | tf_op jit(solution)/shard_map/ppermute | solution.py:14
  171.3 1.5 maximum_convert_fusion
  172.8 6.1 %convolution_convert_fusion.1 = bf16[512,2048]{1,0:T(8,128)(2,1)} fusion(bf16[1024,2048]{1,0:T(8,128)(2,1)} %param.16, f32[514,1024]{1,0:T(8,128)S(1)} %maximum_convert_fusion, bf16[512,1024]{1,0:T(8,128)(2,1)S(1)} %copy-done.6, f32[1024]{0:T(1024)S(1)} %bitcast.54, f32[1024]{0:T(1024)S(1)} %bitcast.55, f32[1024]{0:T(1024)S(1)} %bitcast.53), kind=kOutput, calls=%fused_computation.11 | convolution fusion | flops 2152726528 | bytes 13643776 | tf_op jit(solution)/shard_map/dot_general | solution.py:51
  179.0 3.3 %gather_fusion = bf16[512,2048]{1,0:T(8,128)(2,1)} fusion(bf16[768,2048]{1,0:T(8,128)(2,1)S(1)} %bitcast.46, s32[1024]{0:T(1024)S(1)} %pad_clamp_fusion), kind=kCustom, calls=%fused_computation | custom fusion | bytes 4196352 | tf_op jit(solution)/shard_map/gather | solution.py:87
  182.3 4.8 %reshape.88 = f32[128,4,2048]{2,1,0:T(4,128)} reshape(bf16[512,2048]{1,0:T(8,128)(2,1)} %gather_fusion) | data formatting | bytes 6291456 | tf_op jit(solution)/shard_map/convert_element_type | solution.py:87
  187.0 6.2 %multiply_reduce_fusion = bf16[128,2048]{1,0:T(8,128)(2,1)} fusion(f32[128,4,2048]{2,1,0:T(4,128)} %reshape.88, f32[128,4]{1,0:T(8,128)S(1)} %copy.26), kind=kLoop, calls=%fused_computation.7 | loop fusion | flops 1835008 | bytes 4720640 | tf_op jit(solution)/shard_map/reduce_sum | solution.py:89
  (28 shorter events, 0.4 us)
Async XLA Ops:
  7.0 74.9 %copy-start.3 = (bf16[1,2048,1024]{2,1,0:T(8,128)(2,1)S(1)}, bf16[1,2048,1024]{2,1,0:T(8,128)(2,1)}, u32[]{:S(2)}) copy-start(bf16[1,2048,1024]{2,1,0:T(8,128)(2,1)} %param.21) | copy-start | bytes 12582916
  81.9 3.4 %copy-start.4 = (bf16[1,2048,1024]{2,1,0:T(8,128)(2,1)S(1)}, bf16[1,2048,1024]{2,1,0:T(8,128)(2,1)}, u32[]{:S(2)}) copy-start(bf16[1,2048,1024]{2,1,0:T(8,128)(2,1)} %param.22) | copy-start | bytes 12582916
  85.3 4.0 %copy-start.5 = (bf16[1,1024,2048]{2,1,0:T(8,128)(2,1)S(1)}, bf16[1,1024,2048]{2,1,0:T(8,128)(2,1)}, u32[]{:S(2)}) copy-start(bf16[1,1024,2048]{2,1,0:T(8,128)(2,1)} %param.23) | copy-start | bytes 12582916
  94.2 84.8 %all-to-all-start.1 = ((bf16[32,24,2048]{2,1,0:T(8,128)(2,1)}), bf16[32,24,2048]{2,1,0:T(8,128)(2,1)S(1)}, u32[]{:S(2)}, u32[]{:S(2)}) async-start(bf16[32,24,2048]{2,1,0:T(8,128)(2,1)} %bitcast.48), calls=%async_computation.1 | async-start | bytes 6291456 | tf_op jit(solution)/shard_map/all_to_all | solution.py:82
  99.8 5.3 %copy-start.2 = (f32[128,4]{0,1:T(4,128)S(1)}, f32[128,4]{0,1:T(4,128)}, u32[]{:S(2)}) copy-start(f32[128,4]{0,1:T(4,128)} %param.20) | copy-start | bytes 6148
  99.8 5.3 %copy-start.1 = (f32[3,1024]{1,0:T(4,128)S(1)}, f32[3,1024]{1,0:T(4,128)}, u32[]{:S(2)}) copy-start(f32[3,1024]{1,0:T(4,128)} %param.15) | copy-start | bytes 36868
  101.8 1.0 copy-start
  102.8 68.5 %collective-permute-start = (bf16[2,1024]{1,0:T(2,128)(2,1)S(1)}, bf16[2,1024]{1,0:T(2,128)(2,1)S(1)}, u32[]{:S(2)}, u32[]{:S(2)}) collective-permute-start(bf16[2,1024]{1,0:T(2,128)(2,1)S(1)} %slice.38), channel_id=1, source_target_pairs={{0,1},{1,2},{2,3},{3,4},{4,5},{5,6},{6,7},{7,8},{8,9},{9,10},{10,1... | collective-permute-start | bytes 12296 | tf_op jit(solution)/shard_map/ppermute | solution.py:14
  105.3 67.5 %copy-start.6 = (bf16[512,1024]{1,0:T(8,128)(2,1)S(1)}, bf16[512,1024]{1,0:T(8,128)(2,1)}, u32[]{:S(2)}) copy-start(bf16[512,1024]{1,0:T(8,128)(2,1)} %param.12) | copy-start | bytes 3145732
where the time goes:
time: 194 us; the launch traced here: 193 us
  blocking collectives  74.9 us (39%)
  waiting for transfers between devices  66 us (34%)
  matrix products  20.5 us (11%)
  other arithmetic  12.5 us (6%)
  local copies, waits for them, and re-layouts  10.7 us (6%)
  starting transfers between devices  7.84 us (4%)
    all_to_all x1, blocking collectives, shards(): lax.all_to_all(send_rows, ('ep', 'tp'), split_axis=0, concat_axis=0, tile...  74.9 us
    ppermute x1, waiting for transfers between devices, from_behind(): return lax.ppermute(value, axis, pairs)  66 us
    reduce_sum x1, other arithmetic, shards(): jnp.sum(picked * mix_weight[:, :, None], axis=1).astype(jnp.bfloat16)  6.2 us
    dot_general x1, matrix products, shards(): jnp.dot(gated_rows, mixer_out_weight, preferred_element_type=jnp.float32)  6.14 us
    all_to_all x1, starting transfers between devices, shards(): lax.all_to_all(expert_out.reshape(received.shape), ('ep', 'tp'), split_ax...  5.63 us
    dot_general x1, matrix products, expert_rows(): jnp.dot(hidden, down_weight, preferred_element_type=jnp.float32)  4.81 us
    convert_element_type x1, local copies, waits for them, and re-layouts, shards(): flat_rows[slot_index.reshape(-1)].astype(jnp.float32)  4.75 us
    dot_general x1, matrix products, expert_rows(): up_pre = jnp.dot(row_block, up_weight, preferred_element_type=jnp.float32)  4.02 us
  transfers between devices with their start and end apart: 2, of which 1 were waited for; matrix products, arithmetic and copies ran while one was open for 5% of the time, Pallas kernels for 0%

commit v1 on v0

v1 whole, which is shorter than its diff:
```python
import jax
import jax.numpy as jnp
from jax import lax
from jax.sharding import Mesh, PartitionSpec as P

epsilon = 1e-06
clamp_limit = 7.0
alpha_gate = 1.702
EVERY = ("half", "near", "tp")
NEAR = ("near", "tp")


def from_behind(value, axis, by):
    length = lax.axis_size(axis)
    pairs = [(i, i + by) for i in range(length) if 0 <= i + by < length]
    return lax.ppermute(value, axis, pairs)


def swap_halves(value):
    length = lax.axis_size("half")
    return lax.ppermute(value, "half", [(i, (i + 1) % length) for i in range(length)])


def expert_rows(row_block, gate_weight, up_weight, down_weight):
    gate_pre = jnp.dot(row_block, gate_weight, preferred_element_type=jnp.float32)
    up_pre = jnp.dot(row_block, up_weight, preferred_element_type=jnp.float32)
    gate_pre = jnp.minimum(gate_pre, clamp_limit)
    up_pre = jnp.clip(up_pre, -clamp_limit, clamp_limit)
    hidden = ((up_pre + 1.0) * (gate_pre * jax.nn.sigmoid(alpha_gate * gate_pre))).astype(
        jnp.bfloat16
    )
    return jnp.dot(hidden, down_weight, preferred_element_type=jnp.float32).astype(jnp.bfloat16)


def norm_rows(tokens, norm_gain):
    widened = tokens.astype(jnp.float32)
    return (
        widened
        * lax.rsqrt(jnp.mean(widened * widened, axis=-1, keepdims=True) + epsilon)
        * norm_gain[None, :]
    ).astype(jnp.bfloat16)


def slot_maps(routing, first_expert, experts_near, capacity):
    top_count = routing.shape[0] // 2
    tokens = routing.shape[1]
    ids = routing[:top_count].astype(jnp.int32)
    weights = routing[top_count:]
    mix_weight = weights / jnp.sum(weights, axis=0, keepdims=True)
    experts = first_expert + lax.broadcasted_iota(jnp.int32, (experts_near, 1), 0)
    named = jnp.zeros((experts_near, tokens), jnp.float32)
    share = jnp.zeros((experts_near, tokens), jnp.float32)
    for choice in range(top_count):
        hit = ids[choice][None, :] == experts
        named = named + hit.astype(jnp.float32)
        share = share + jnp.where(hit, mix_weight[choice][None, :], 0.0)
    before = lax.broadcasted_iota(jnp.int32, (tokens, tokens), 0) < lax.broadcasted_iota(
        jnp.int32, (tokens, tokens), 1
    )
    rank = jnp.dot(
        named.astype(jnp.bfloat16), before.astype(jnp.bfloat16), preferred_element_type=jnp.float32
    )
    slots = lax.broadcasted_iota(jnp.int32, (experts_near, capacity, tokens), 1)
    rank = jnp.where(named > 0, rank.astype(jnp.int32), capacity)
    here = rank[:, None, :] == slots
    dispatch = here.astype(jnp.bfloat16).reshape(experts_near * capacity, tokens)
    combine = jnp.where(here, share[:, None, :], 0.0).reshape(experts_near * capacity, tokens)
    return dispatch, combine


def to_experts(dispatch, rows, members):
    send = jnp.dot(dispatch, rows, preferred_element_type=jnp.float32).astype(jnp.bfloat16)
    send = send.reshape(members, -1, rows.shape[1])
    return lax.all_to_all(send, NEAR, split_axis=0, concat_axis=0, tiled=True)


def from_experts(combine, rows, received_shape):
    back = lax.all_to_all(
        rows.reshape(received_shape), NEAR, split_axis=0, concat_axis=0, tiled=True
    ).reshape(rows.shape)
    high = lax.reduce_precision(combine, 8, 7)
    low = combine - high
    total = None
    for part in (high, low):
        term = lax.dot_general(
            part.astype(jnp.bfloat16),
            back,
            (((0,), (0,)), ((), ())),
            preferred_element_type=jnp.float32,
        )
        total = term if total is None else total + term
    return total


def shards(
    gate_outer,
    gate_inner,
    conv_input,
    conv_taps,
    mixer_out_weight,
    moe_tokens,
    norm_gain,
    expert_ids,
    route_weight,
    expert_gate,
    expert_up,
    expert_down,
):
    tokens_here, width = moe_tokens.shape
    top_count = expert_ids.shape[1]
    experts_near = lax.axis_size(NEAR)
    experts_all = lax.axis_size(EVERY)
    capacity = 3 * tokens_here * top_count // (2 * experts_all)
    first_expert = lax.axis_index("half") * experts_near

    routing = jnp.concatenate([expert_ids.T.astype(jnp.float32), route_weight.T], 0)
    far_routing = swap_halves(routing)
    far_tokens = swap_halves(moe_tokens)

    dispatch, combine = slot_maps(routing, first_expert, experts_near, capacity)
    received = to_experts(dispatch, norm_rows(moe_tokens, norm_gain), experts_near)

    reach_rows = conv_taps.shape[0] - 1
    rows_here = gate_inner.shape[0]
    product = (gate_inner.astype(jnp.float32) * conv_input.astype(jnp.float32)).astype(jnp.bfloat16)
    previous = from_behind(product[rows_here - reach_rows :], EVERY, 1)
    extended = jnp.concatenate([previous, product], 0).astype(jnp.float32)
    convolved = jnp.zeros(product.shape, jnp.float32)
    for offset in range(conv_taps.shape[0]):
        convolved = convolved + conv_taps[offset][None, :] * extended[offset : offset + rows_here]
    gated_rows = (gate_outer.astype(jnp.float32) * convolved).astype(jnp.bfloat16)
    mixed_out = jnp.dot(
        gated_rows, mixer_out_weight, preferred_element_type=jnp.float32
    ).astype(jnp.bfloat16)

    far_dispatch, far_combine = slot_maps(far_routing, first_expert, experts_near, capacity)
    far_received = to_experts(far_dispatch, norm_rows(far_tokens, norm_gain), experts_near)

    expert_out = expert_rows(
        received.reshape(-1, width), expert_gate[0], expert_up[0], expert_down[0]
    )
    far_out = expert_rows(
        far_received.reshape(-1, width), expert_gate[0], expert_up[0], expert_down[0]
    )
    far_total = from_experts(far_combine, far_out, received.shape).astype(jnp.bfloat16)
    returned = swap_halves(far_total)
    total = from_experts(combine, expert_out, received.shape)
    moe_out = (total + returned.astype(jnp.float32)).astype(jnp.bfloat16)
    return (mixed_out, moe_out)


def solution(mesh):
    outer, inner = mesh.shape["ep"], mesh.shape["tp"]
    halves = 2 if outer % 2 == 0 else 1
    split = Mesh(mesh.devices.reshape(halves, outer // halves, inner), EVERY)
    rows = P(EVERY, None)
    weights = P(EVERY, None, None)
    in_specs = (rows, rows, rows, P(), P(), rows, P(), rows, rows, weights, weights, weights)
    return jax.shard_map(
        shards, mesh=split, in_specs=in_specs, out_specs=(rows, rows), check_vma=False
    )
```

time: 194 us -> 167 us (0.86)
  the two profiles are of different devices: /device:TPU:16 before, /device:TPU:3 now
where the time goes in v1:
time: 167 us
  waiting for transfers between devices  86.8 us (52%)
  matrix products  37.7 us (23%)
  starting transfers between devices  34.6 us (21%)
  other arithmetic  5.5 us (3%)
    ppermute x3, waiting for transfers between devices, swap_halves(): lax.ppermute(value, 'half', [(i, (i + 1) % length) for i in range(length)])  43.9 us
    all_to_all x2, waiting for transfers between devices, to_experts(): return lax.all_to_all(send, NEAR, split_axis=0, concat_axis=0, tiled=True)  24.7 us
    dot_general x2, matrix products, expert_rows(): jnp.dot(hidden, down_weight, preferred_element_type=jnp.float32)  17.1 us
    all_to_all x2, starting transfers between devices, from_experts(): lax.all_to_all(rows.reshape(received_shape), NEAR, split_axis=0, concat_a...  14 us
    all_to_all x2, starting transfers between devices, to_experts(): return lax.all_to_all(send, NEAR, split_axis=0, concat_axis=0, tiled=True)  12.8 us
    ppermute x1, waiting for transfers between devices, from_behind(): return lax.ppermute(value, axis, pairs)  12 us
    dot_general x2, matrix products, expert_rows(): jnp.dot(row_block, gate_weight, preferred_element_type=jnp.float32)  8.42 us
    all_to_all x2, waiting for transfers between devices, from_experts(): lax.all_to_all(rows.reshape(received_shape), NEAR, split_axis=0, concat_a...  6.25 us
  transfers between devices with their start and end apart: 8, of which 7 were waited for; matrix products, arithmetic and copies ran while one was open for 23% of the time, Pallas kernels for 0%

profile of v1, /device:TPU:3, one launch (start us, length us, event | category | flops | bytes accessed | tf_op | source)
XLA Modules:
  0.0 166.6 jit_solution(4577956846803925090)
XLA Ops:
  2.0 2.3 %collective-permute-start.1 = (f32[8,128]{1,0:T(8,128)S(1)}, f32[8,128]{1,0:T(8,128)S(1)}, u32[]{:S(2)}, u32[]{:S(2)}) collective-permute-start(f32[8,128]{1,0:T(8,128)S(1)} %pad_maximum_fusion), channel_id=1, source_target_pairs={{0,16},{16,0},{1,17},{17,1},{2,18},{18,2},{3,19},{19,3},{4,20},{20... | collective-permute-start | bytes 12296 | tf_op jit(solution)/shard_map/ppermute | solution.py:21
  5.7 23.8 %collective-permute-done.2 = bf16[128,2048]{1,0:T(8,128)(2,1)S(1)} collective-permute-done((bf16[128,2048]{1,0:T(8,128)(2,1)}, bf16[128,2048]{1,0:T(8,128)(2,1)S(1)}, u32[]{:S(2)}, u32[]{:S(2)}) %collective-permute-start.2) | collective-permute-done | bytes 524320 | tf_op jit(solution)/shard_map/ppermute | solution.py:21
  29.7 2.5 %convolution_convert_fusion.1 = bf16[384,2048]{1,0:T(8,128)(2,1)} fusion(pred[384,128]{1,0:T(32,128)(4,1)S(1)} %get-tuple-element.12, bf16[128,2048]{1,0:T(8,128)(2,1)S(1)} %collective-permute-done.2, f32[128]{0:T(128)S(1)} %add_rsqrt_fusion, f32[2048]{0:T(1024)} %param.18), kind=kOutput, calls=%fused_computation.15 | convolution fusion | flops 203161600 | bytes 2155008 | tf_op jit(solution)/shard_map/dot_general | solution.py:72
  32.2 5.5 %all-to-all-start.2 = ((bf16[16,24,2048]{2,1,0:T(8,128)(2,1)}), bf16[16,24,2048]{2,1,0:T(8,128)(2,1)S(1)}, u32[]{:S(2)}, u32[]{:S(2)}) async-start(bf16[16,24,2048]{2,1,0:T(8,128)(2,1)} %bitcast.31), calls=%async_computation.2 | async-start | bytes 3145728 | tf_op jit(solution)/shard_map/all_to_all | solution.py:74
  37.9 1.8 %convolution_convert_fusion.2 = bf16[384,2048]{1,0:T(8,128)(2,1)} fusion(pred[384,128]{1,0:T(32,128)(4,1)S(1)} %get-tuple-element.11, bf16[128,2048]{1,0:T(8,128)(2,1)S(1)} %copy-done.1, f32[2048]{0:T(1024)S(1)} %copy-done.2, f32[128]{0:T(128)S(1)} %add_rsqrt_fusion.1), kind=kOutput, calls=%fused_computation.16 | convolution fusion | flops 203161600 | bytes 2155008 | tf_op jit(solution)/shard_map/dot_general | solution.py:72
  39.7 17.5 %all-to-all-done.2 = bf16[16,24,2048]{2,1,0:T(8,128)(2,1)S(1)} async-done(((bf16[16,24,2048]{2,1,0:T(8,128)(2,1)}), bf16[16,24,2048]{2,1,0:T(8,128)(2,1)S(1)}, u32[]{:S(2)}, u32[]{:S(2)}) %all-to-all-start.2) | async-done | bytes 1572896 | tf_op jit(solution)/shard_map/all_to_all | solution.py:74
  57.2 7.3 %all-to-all-start = ((bf16[16,24,2048]{2,1,0:T(8,128)(2,1)}), bf16[16,24,2048]{2,1,0:T(8,128)(2,1)}, u32[]{:S(2)}, u32[]{:S(2)}) async-start(bf16[16,24,2048]{2,1,0:T(8,128)(2,1)} %bitcast.14), calls=%async_computation | async-start | bytes 3145728 | tf_op jit(solution)/shard_map/all_to_all | solution.py:74
  64.5 4.0 %fusion.4 = f32[384,1024]{1,0:T(8,128)S(1)} fusion(bf16[384,2048]{1,0:T(8,128)(2,1)S(1)} %bitcast.106, bf16[1,2048,1024]{2,1,0:T(8,128)(2,1)} %param.21), kind=kOutput, calls=%fused_computation.4 | convolution fusion | flops 1610612736 | bytes 7340032 | tf_op jit(solution)/shard_map/dot_general | solution.py:25
  68.4 8.3 %fusion.15 = bf16[384,2048]{1,0:T(8,128)(2,1)} fusion(bf16[1,1024,2048]{2,1,0:T(8,128)(2,1)} %param.23, f32[384,1024]{1,0:T(8,128)S(1)} %fusion.4, bf16[384,2048]{1,0:T(8,128)(2,1)S(1)} %bitcast.107, bf16[1,2048,1024]{2,1,0:T(8,128)(2,1)} %param.22), kind=kOutput, calls=%fused_computation.14 | convolution fusion | flops 3225944064 | bytes 13107200 | tf_op jit(solution)/shard_map/dot_general | solution.py:32
  76.7 7.3 %all-to-all-done = bf16[16,24,2048]{2,1,0:T(8,128)(2,1)} async-done(((bf16[16,24,2048]{2,1,0:T(8,128)(2,1)}), bf16[16,24,2048]{2,1,0:T(8,128)(2,1)}, u32[]{:S(2)}, u32[]{:S(2)}) %all-to-all-start) | async-done | bytes 1572896 | tf_op jit(solution)/shard_map/all_to_all | solution.py:74
  84.0 7.0 %all-to-all-start.3 = ((bf16[16,24,2048]{2,1,0:T(8,128)(2,1)}), bf16[16,24,2048]{2,1,0:T(8,128)(2,1)S(1)}, u32[]{:S(2)}, u32[]{:S(2)}) async-start(bf16[16,24,2048]{2,1,0:T(8,128)(2,1)} %bitcast.108), calls=%async_computation.3 | async-start | bytes 3145728 | tf_op jit(solution)/shard_map/all_to_all | solution.py:78
  91.0 4.4 %fusion.6 = f32[384,1024]{1,0:T(8,128)S(1)} fusion(bf16[384,2048]{1,0:T(8,128)(2,1)} %bitcast.15, bf16[1,2048,1024]{2,1,0:T(8,128)(2,1)} %param.21), kind=kOutput, calls=%fused_computation.6 | convolution fusion | flops 1610612736 | bytes 7340032 | tf_op jit(solution)/shard_map/dot_general | solution.py:25
  95.5 8.8 %fusion.12 = bf16[384,2048]{1,0:T(8,128)(2,1)} fusion(bf16[1,1024,2048]{2,1,0:T(8,128)(2,1)} %param.23, f32[384,1024]{1,0:T(8,128)S(1)} %fusion.6, bf16[384,2048]{1,0:T(8,128)(2,1)} %bitcast.15, bf16[1,2048,1024]{2,1,0:T(8,128)(2,1)} %param.22), kind=kOutput, calls=%fused_computation.13 | convolution fusion | flops 3225944064 | bytes 13107200 | tf_op jit(solution)/shard_map/dot_general | solution.py:32
  104.2 6.2 %all-to-all-done.3 = bf16[16,24,2048]{2,1,0:T(8,128)(2,1)S(1)} async-done(((bf16[16,24,2048]{2,1,0:T(8,128)(2,1)}), bf16[16,24,2048]{2,1,0:T(8,128)(2,1)S(1)}, u32[]{:S(2)}, u32[]{:S(2)}) %all-to-all-start.3) | async-done | bytes 1572896 | tf_op jit(solution)/shard_map/all_to_all | solution.py:78
  110.5 7.0 %all-to-all-start.1 = ((bf16[16,24,2048]{2,1,0:T(8,128)(2,1)}), bf16[16,24,2048]{2,1,0:T(8,128)(2,1)S(1)}, u32[]{:S(2)}, u32[]{:S(2)}) async-start(bf16[16,24,2048]{2,1,0:T(8,128)(2,1)} %bitcast.105), calls=%async_computation.1 | async-start | bytes 3145728 | tf_op jit(solution)/shard_map/all_to_all | solution.py:78
  117.5 1.9 %multiply_convert_fusion = bf16[512,1024]{1,0:T(8,128)(2,1)S(1)} fusion(bf16[512,1024]{1,0:T(8,128)(2,1)} %param.14, bf16[512,1024]{1,0:T(8,128)(2,1)} %param.13), kind=kLoop, calls=%fused_computation.31 | loop fusion | flops 2097152 | bytes 3145728 | tf_op jit(solution)/shard_map/convert_element_type | solution.py:125
  120.4 3.6 %collective-permute-start = (bf16[2,1024]{1,0:T(2,128)(2,1)S(1)}, bf16[2,1024]{1,0:T(2,128)(2,1)S(1)}, u32[]{:S(2)}, u32[]{:S(2)}) collective-permute-start(bf16[2,1024]{1,0:T(2,128)(2,1)S(1)} %slice.100), channel_id=1, source_target_pairs={{0,1},{1,2},{2,3},{3,4},{4,5},{5,6},{6,7},{7,8},{8,9},{9,10},{10,1... | collective-permute-start | bytes 12296 | tf_op jit(solution)/shard_map/ppermute | solution.py:16
  124.0 12.0 %collective-permute-done = bf16[2,1024]{1,0:T(2,128)(2,1)S(1)} collective-permute-done((bf16[2,1024]{1,0:T(2,128)(2,1)S(1)}, bf16[2,1024]{1,0:T(2,128)(2,1)S(1)}, u32[]{:S(2)}, u32[]{:S(2)}) %collective-permute-start) | collective-permute-done | bytes 4128 | tf_op jit(solution)/shard_map/ppermute | solution.py:16
  136.0 1.5 maximum_convert_fusion
  138.2 1.3 fusion.20
  139.4 1.9 %collective-permute-start.3 = (bf16[128,2048]{1,0:T(8,128)(2,1)}, bf16[128,2048]{1,0:T(8,128)(2,1)S(1)}, u32[]{:S(2)}, u32[]{:S(2)}) collective-permute-start(bf16[128,2048]{1,0:T(8,128)(2,1)} %fusion.20), channel_id=1, source_target_pairs={{0,16},{16,0},{1,17},{17,1},{2,18},{18,2},{3,19},{19,3},{4,20},{20... | collective-permute-start | bytes 1572872 | tf_op jit(solution)/shard_map/ppermute | solution.py:21
  141.4 4.0 %convolution_convert_fusion = bf16[512,2048]{1,0:T(8,128)(2,1)} fusion(bf16[1024,2048]{1,0:T(8,128)(2,1)S(1)} %copy-done.5, f32[514,1024]{1,0:T(8,128)S(1)} %maximum_convert_fusion, bf16[512,1024]{1,0:T(8,128)(2,1)S(1)} %copy-done.6, f32[1024]{0:T(1024)S(1)} %bitcast.111, f32[1024]{0:T(1024)S(1)} %bitcast.112, f32[1024]{0:T(1024)S(1)} %bitcast.110), kind=kOutput, calls=%fused_computation.12 | convolution fusion | flops 2152726528 | bytes 13643776 | tf_op jit(solution)/shard_map/dot_general | solution.py:132
  145.9 19.4 %collective-permute-done.3 = bf16[128,2048]{1,0:T(8,128)(2,1)S(1)} collective-permute-done((bf16[128,2048]{1,0:T(8,128)(2,1)}, bf16[128,2048]{1,0:T(8,128)(2,1)S(1)}, u32[]{:S(2)}, u32[]{:S(2)}) %collective-permute-start.3) | collective-permute-done | bytes 524320 | tf_op jit(solution)/shard_map/ppermute | solution.py:21
  165.3 1.3 add_convert_fusion
  (42 shorter events, 5.2 us)
Async XLA Ops:
  2.0 3.4 %collective-permute-start.1 = (f32[8,128]{1,0:T(8,128)S(1)}, f32[8,128]{1,0:T(8,128)S(1)}, u32[]{:S(2)}, u32[]{:S(2)}) collective-permute-start(f32[8,128]{1,0:T(8,128)S(1)} %pad_maximum_fusion), channel_id=1, source_target_pairs={{0,16},{16,0},{1,17},{17,1},{2,18},{18,2},{3,19},{19,3},{4,20},{20... | collective-permute-start | bytes 12296 | tf_op jit(solution)/shard_map/ppermute | solution.py:21
  4.3 25.2 %collective-permute-start.2 = (bf16[128,2048]{1,0:T(8,128)(2,1)}, bf16[128,2048]{1,0:T(8,128)(2,1)S(1)}, u32[]{:S(2)}, u32[]{:S(2)}) collective-permute-start(bf16[128,2048]{1,0:T(8,128)(2,1)} %param.17), channel_id=1, source_target_pairs={{0,16},{16,0},{1,17},{17,1},{2,18},{18,2},{3,19},{19,3},{4,20},{20... | collective-permute-start | bytes 1572872 | tf_op jit(solution)/shard_map/ppermute | solution.py:21
  32.2 5.5 %copy-start.1 = (bf16[128,2048]{1,0:T(8,128)(2,1)S(1)}, bf16[128,2048]{1,0:T(8,128)(2,1)}, u32[]{:S(2)}) copy-start(bf16[128,2048]{1,0:T(8,128)(2,1)} %param.17) | copy-start | bytes 1572868
  32.2 5.7 %copy-start.2 = (f32[2048]{0:T(1024)S(1)}, f32[2048]{0:T(1024)}, u32[]{:S(2)}) copy-start(f32[2048]{0:T(1024)} %param.18) | copy-start | bytes 24580
  32.2 25.0 %all-to-all-start.2 = ((bf16[16,24,2048]{2,1,0:T(8,128)(2,1)}), bf16[16,24,2048]{2,1,0:T(8,128)(2,1)S(1)}, u32[]{:S(2)}, u32[]{:S(2)}) async-start(bf16[16,24,2048]{2,1,0:T(8,128)(2,1)} %bitcast.31), calls=%async_computation.2 | async-start | bytes 3145728 | tf_op jit(solution)/shard_map/all_to_all | solution.py:74
  57.2 26.8 %all-to-all-start = ((bf16[16,24,2048]{2,1,0:T(8,128)(2,1)}), bf16[16,24,2048]{2,1,0:T(8,128)(2,1)}, u32[]{:S(2)}, u32[]{:S(2)}) async-start(bf16[16,24,2048]{2,1,0:T(8,128)(2,1)} %bitcast.14), calls=%async_computation | async-start | bytes 3145728 | tf_op jit(solution)/shard_map/all_to_all | solution.py:74
  84.0 26.5 %all-to-all-start.3 = ((bf16[16,24,2048]{2,1,0:T(8,128)(2,1)}), bf16[16,24,2048]{2,1,0:T(8,128)(2,1)S(1)}, u32[]{:S(2)}, u32[]{:S(2)}) async-start(bf16[16,24,2048]{2,1,0:T(8,128)(2,1)} %bitcast.108), calls=%async_computation.3 | async-start | bytes 3145728 | tf_op jit(solution)/shard_map/all_to_all | solution.py:78
  110.5 34.9 %all-to-all-start.1 = ((bf16[16,24,2048]{2,1,0:T(8,128)(2,1)}), bf16[16,24,2048]{2,1,0:T(8,128)(2,1)S(1)}, u32[]{:S(2)}, u32[]{:S(2)}) async-start(bf16[16,24,2048]{2,1,0:T(8,128)(2,1)} %bitcast.105), calls=%async_computation.1 | async-start | bytes 3145728 | tf_op jit(solution)/shard_map/all_to_all | solution.py:78
  117.5 6.5 %copy-start.3 = (f32[128,4]{0,1:T(4,128)S(1)}, f32[128,4]{0,1:T(4,128)}, u32[]{:S(2)}) copy-start(f32[128,4]{0,1:T(4,128)} %param.20) | copy-start | bytes 6148
  117.5 6.5 %copy-start.4 = (f32[3,1024]{1,0:T(4,128)S(1)}, f32[3,1024]{1,0:T(4,128)}, u32[]{:S(2)}) copy-start(f32[3,1024]{1,0:T(4,128)} %param.15) | copy-start | bytes 36868
  119.4 1.0 copy-start
  120.4 15.6 %collective-permute-start = (bf16[2,1024]{1,0:T(2,128)(2,1)S(1)}, bf16[2,1024]{1,0:T(2,128)(2,1)S(1)}, u32[]{:S(2)}, u32[]{:S(2)}) collective-permute-start(bf16[2,1024]{1,0:T(2,128)(2,1)S(1)} %slice.100), channel_id=1, source_target_pairs={{0,1},{1,2},{2,3},{3,4},{4,5},{5,6},{6,7},{7,8},{8,9},{9,10},{10,1... | collective-permute-start | bytes 12296 | tf_op jit(solution)/shard_map/ppermute | solution.py:16
  137.7 3.7 %copy-start.5 = (bf16[1024,2048]{1,0:T(8,128)(2,1)S(1)}, bf16[1024,2048]{1,0:T(8,128)(2,1)}, u32[]{:S(2)}) copy-start(bf16[1024,2048]{1,0:T(8,128)(2,1)} %param.16) | copy-start | bytes 12582916
  138.2 3.2 %copy-start.6 = (bf16[512,1024]{1,0:T(8,128)(2,1)S(1)}, bf16[512,1024]{1,0:T(8,128)(2,1)}, u32[]{:S(2)}) copy-start(bf16[512,1024]{1,0:T(8,128)(2,1)} %param.12) | copy-start | bytes 3145732
  139.4 25.9 %collective-permute-start.3 = (bf16[128,2048]{1,0:T(8,128)(2,1)}, bf16[128,2048]{1,0:T(8,128)(2,1)S(1)}, u32[]{:S(2)}, u32[]{:S(2)}) collective-permute-start(bf16[128,2048]{1,0:T(8,128)(2,1)} %fusion.20), channel_id=1, source_target_pairs={{0,16},{16,0},{1,17},{17,1},{2,18},{18,2},{3,19},{19,3},{4,20},{20... | collective-permute-start | bytes 1572872 | tf_op jit(solution)/shard_map/ppermute | solution.py:21

commit v2 on v0

v2 whole, which is shorter than its diff:
```python
import functools
import math

import jax
import jax.numpy as jnp
from jax import lax
from jax.experimental import pallas as pl
from jax.experimental.pallas import tpu as pltpu
from jax.sharding import Mesh, PartitionSpec as P

epsilon = 1e-06
clamp_limit = 7.0
alpha_gate = 1.702
EVERY = ("half", "near", "tp")
NEAR = ("near", "tp")
SMALL_VMEM = 12 * 1024 * 1024
WIDE_VMEM = 58 * 1024 * 1024
AHEAD = 3


def from_behind(value, axis, by):
    length = lax.axis_size(axis)
    pairs = [(i, i + by) for i in range(length) if 0 <= i + by < length]
    return lax.ppermute(value, axis, pairs)


def swap_halves(value):
    halves, near = lax.axis_size("half"), lax.axis_size("near")
    shift = near // 2 if near % 2 == 0 and halves > 1 else 0
    pairs = [
        (h * near + n, (h + 1) % halves * near + (n + shift) % near)
        for h in range(halves)
        for n in range(near)
    ]
    return lax.ppermute(value, ("half", "near"), pairs)


def dispatch_kernel(
    capacity, masked, place_ref, ids_ref, weight_ref, rows_ref, gain_ref, slot_ref, mix_ref, *send_refs
):
    top_count, tokens = ids_ref.shape
    slots = sum(ref.shape[0] for ref in send_refs)
    experts_near = slots // capacity
    ids = ids_ref[...] - place_ref[0]
    weights = weight_ref[...]
    mix_ref[...] = weights / jnp.sum(weights, axis=0, keepdims=True)
    experts = lax.broadcasted_iota(jnp.int32, (experts_near, tokens), 0)
    hits = [ids[k : k + 1, :] == experts for k in range(top_count)]
    named = functools.reduce(jnp.logical_or, hits)
    before = lax.broadcasted_iota(jnp.int32, (tokens, tokens), 0) < lax.broadcasted_iota(
        jnp.int32, (tokens, tokens), 1
    )
    rank = jnp.dot(
        named.astype(jnp.float32).astype(jnp.bfloat16),
        before.astype(jnp.float32).astype(jnp.bfloat16),
        preferred_element_type=jnp.float32,
    )
    slot_rows = lax.broadcasted_iota(jnp.int32, (slots, tokens), 0)
    here = None
    for k in range(top_count):
        own = jnp.sum(jnp.where(hits[k], rank, 0.0), axis=0, keepdims=True).astype(jnp.int32)
        choice = ids[k : k + 1, :]
        inside = (choice >= 0) & (choice < experts_near)
        block = choice ^ place_ref[1] if masked else choice
        slot = jnp.where(inside, block * capacity + own, slots)
        slot_ref[k : k + 1, :] = slot
        match = slot_rows == slot
        here = match if here is None else here | match
    widened = rows_ref[...].astype(jnp.float32)
    normed = (
        widened
        * lax.rsqrt(jnp.mean(widened * widened, axis=-1, keepdims=True) + epsilon)
        * gain_ref[...]
    ).astype(jnp.bfloat16)
    laid = jnp.dot(
        here.astype(jnp.float32).astype(jnp.bfloat16), normed, preferred_element_type=jnp.float32
    )
    start = 0
    for ref in send_refs:
        ref[...] = laid[start : start + ref.shape[0]].astype(ref.dtype)
        start += ref.shape[0]


def block_shapes(slots, width, blocks):
    return [jax.ShapeDtypeStruct((slots // blocks, width), jnp.bfloat16)] * blocks


def to_slots(place, ids, weights, rows, gain, slots, capacity, blocks, room):
    top_count, tokens = ids.shape
    width = rows.shape[1]
    held = pl.BlockSpec(memory_space=pltpu.VMEM)
    slot, mix, *send = pl.pallas_call(
        functools.partial(dispatch_kernel, capacity, blocks > 1),
        in_specs=[pl.BlockSpec(memory_space=pltpu.SMEM)] + [held] * 4,
        out_specs=[held] * (2 + blocks),
        out_shape=[
            jax.ShapeDtypeStruct((top_count, tokens), jnp.int32),
            jax.ShapeDtypeStruct((top_count, tokens), jnp.float32),
        ]
        + block_shapes(slots, width, blocks),
        compiler_params=pltpu.CompilerParams(vmem_limit_bytes=room),
        cost_estimate=pl.CostEstimate(
            flops=2 * slots * tokens * width,
            bytes_accessed=2 * (slots + tokens) * width,
            transcendentals=tokens,
        ),
    )(place, ids, weights, rows, gain)
    return slot, mix, send


def gather_blocks(refs, wide_ref):
    if len(refs) == 1:
        return refs[0][...]
    start = 0
    for ref in refs:
        wide_ref[start : start + ref.shape[0], :] = ref[...].astype(jnp.float32)
        start += ref.shape[0]
    return wide_ref[...].astype(jnp.bfloat16)


def combine_kernel(blocks, addends, slot_ref, mix_ref, *refs):
    back_refs, add_refs = refs[:blocks], refs[blocks : blocks + addends]
    out_ref, wide_ref = refs[blocks + addends :]
    slots = sum(ref.shape[0] for ref in back_refs)
    top_count, tokens = slot_ref.shape
    slot_rows = lax.broadcasted_iota(jnp.int32, (slots, tokens), 0)
    share = jnp.zeros((slots, tokens), jnp.float32)
    for k in range(top_count):
        share = jnp.where(slot_rows == slot_ref[k : k + 1, :], mix_ref[k : k + 1, :], share)
    high = share.astype(jnp.bfloat16)
    low = (share - high.astype(jnp.float32)).astype(jnp.bfloat16)
    back = gather_blocks(back_refs, wide_ref)
    over = (((0,), (0,)), ((), ()))
    total = lax.dot_general(high, back, over, preferred_element_type=jnp.float32)
    total = total + lax.dot_general(low, back, over, preferred_element_type=jnp.float32)
    for ref in add_refs:
        total = total + ref[...].astype(jnp.float32)
    out_ref[...] = total.astype(out_ref.dtype)


def from_slots(slot, mix, back, addends):
    slots, width = sum(block.shape[0] for block in back), back[0].shape[1]
    tokens = slot.shape[1]
    wide = (slots, width) if len(back) > 1 else (8, 128)
    return pl.pallas_call(
        functools.partial(combine_kernel, len(back), len(addends)),
        in_specs=[pl.BlockSpec(memory_space=pltpu.VMEM)] * (2 + len(back) + len(addends)),
        out_specs=pl.BlockSpec(memory_space=pltpu.VMEM),
        out_shape=jax.ShapeDtypeStruct((tokens, width), jnp.bfloat16),
        scratch_shapes=[pltpu.VMEM(wide, jnp.float32)],
        compiler_params=pltpu.CompilerParams(vmem_limit_bytes=SMALL_VMEM),
        cost_estimate=pl.CostEstimate(
            flops=4 * slots * tokens * width,
            bytes_accessed=2 * (slots + tokens) * width,
            transcendentals=0,
        ),
    )(slot, mix, *back, *addends)


def expert_kernel(blocks, gate, up, down, *refs):
    in_refs, out_refs = refs[:blocks], refs[blocks : 2 * blocks]
    gate_ref, up_ref, down_ref, hidden_ref, wide_ref, sems = refs[2 * blocks :]
    parts, _, tile = gate_ref.shape
    columns, _, column = down_ref.shape
    work = []
    for part in range(parts):
        cut = pl.ds(part * tile, tile)
        work.append(((gate, gate_ref, part, cut), (up, up_ref, part, cut)))
    for part in range(columns):
        work.append(((down, down_ref, part, pl.ds(part * column, column)),))
    copies = [
        [
            pltpu.make_async_copy(source.at[0, :, cut], target.at[part], sems.at[step, at])
            for at, (source, target, part, cut) in enumerate(pieces)
        ]
        for step, pieces in enumerate(work)
    ]

    def ready(step):
        for copy in copies[step]:
            copy.wait()
        if step + AHEAD < len(copies):
            for copy in copies[step + AHEAD]:
                copy.start()

    for step in range(min(AHEAD, len(copies))):
        for copy in copies[step]:
            copy.start()
    rows = gather_blocks(in_refs, wide_ref)
    for part in range(parts):
        ready(part)
        gate_pre = jnp.dot(rows, gate_ref[part], preferred_element_type=jnp.float32)
        up_pre = jnp.dot(rows, up_ref[part], preferred_element_type=jnp.float32)
        gate_pre = jnp.minimum(gate_pre, clamp_limit)
        up_pre = jnp.clip(up_pre, -clamp_limit, clamp_limit)
        hidden_ref[:, part * tile : (part + 1) * tile] = (
            (up_pre + 1.0) * (gate_pre * jax.nn.sigmoid(alpha_gate * gate_pre))
        ).astype(jnp.bfloat16)
    for part in range(columns):
        ready(parts + part)
        result = jnp.dot(hidden_ref[...], down_ref[part], preferred_element_type=jnp.float32)
        start = 0
        for ref in out_refs:
            ref[:, part * column : (part + 1) * column] = result[
                start : start + ref.shape[0]
            ].astype(ref.dtype)
            start += ref.shape[0]


def expert_rows(rows, weights):
    count, width = sum(block.shape[0] for block in rows), rows[0].shape[1]
    hidden = weights[0].shape[2]
    tile, column = math.gcd(hidden, 256), math.gcd(width, 512)
    parts, columns = hidden // tile, width // column
    held = pl.BlockSpec(memory_space=pltpu.VMEM)
    wide = (count, width) if len(rows) > 1 else (8, 128)
    return pl.pallas_call(
        functools.partial(expert_kernel, len(rows)),
        in_specs=[pl.BlockSpec(memory_space=pl.ANY)] * 3 + [held] * len(rows),
        out_specs=[held] * len(rows),
        out_shape=block_shapes(count, width, len(rows)),
        scratch_shapes=[
            pltpu.VMEM((parts, width, tile), jnp.bfloat16),
            pltpu.VMEM((parts, width, tile), jnp.bfloat16),
            pltpu.VMEM((columns, hidden, column), jnp.bfloat16),
            pltpu.VMEM((count, hidden), jnp.bfloat16),
            pltpu.VMEM(wide, jnp.float32),
            pltpu.SemaphoreType.DMA((parts + columns, 2)),
        ],
        compiler_params=pltpu.CompilerParams(vmem_limit_bytes=WIDE_VMEM),
        cost_estimate=pl.CostEstimate(
            flops=6 * count * width * hidden,
            bytes_accessed=2 * (3 * width * hidden + 2 * count * width),
            transcendentals=count * hidden,
        ),
    )(*weights, *rows)


def hop_order(members):
    ranked = sorted(range(2, members), key=lambda mask: bin(mask >> 1).count("1"))
    mixed = []
    while ranked:
        mixed.append(ranked.pop())
        if ranked:
            mixed.append(ranked.pop(0))
    return mixed + [1] * (members > 1)


def hops(blocks, masks):
    members = len(blocks)
    arrived = {
        mask: lax.ppermute(blocks[mask], NEAR, [(i, i ^ mask) for i in range(members)])
        for mask in masks
    }
    return arrived


def in_order(first, arrived):
    return [first] + [arrived[mask] for mask in sorted(arrived)]


def exchange(rows, members):
    parts = rows.reshape(members, -1, rows.shape[1])
    return lax.all_to_all(parts, NEAR, split_axis=0, concat_axis=0, tiled=True).reshape(rows.shape)


def gated_input(gate_inner, conv_input):
    return (gate_inner.astype(jnp.float32) * conv_input.astype(jnp.float32)).astype(jnp.bfloat16)


def mixer(gate_outer, gate_inner, conv_input, previous, conv_taps, mixer_out_weight):
    rows_here = gate_inner.shape[0]
    product = gated_input(gate_inner, conv_input)
    extended = jnp.concatenate([previous, product], 0).astype(jnp.float32)
    convolved = jnp.zeros(product.shape, jnp.float32)
    for offset in range(conv_taps.shape[0]):
        convolved = convolved + conv_taps[offset][None, :] * extended[offset : offset + rows_here]
    gated_rows = (gate_outer.astype(jnp.float32) * convolved).astype(jnp.bfloat16)
    return jnp.dot(gated_rows, mixer_out_weight, preferred_element_type=jnp.float32).astype(
        jnp.bfloat16
    )


def shards(
    gate_outer,
    gate_inner,
    conv_input,
    conv_taps,
    mixer_out_weight,
    moe_tokens,
    norm_gain,
    expert_ids,
    route_weight,
    expert_gate,
    expert_up,
    expert_down,
):
    tokens_here, top_count = expert_ids.shape
    members = lax.axis_size(NEAR)
    capacity = 3 * tokens_here * top_count // (2 * lax.axis_size(EVERY))
    capacity = -(-capacity // 8) * 8
    slots = members * capacity
    masks = hop_order(members)
    place = jnp.stack([lax.axis_index("half") * members, lax.axis_index(NEAR)])
    gain = norm_gain[None, :]
    ids, route = expert_ids.T, route_weight.T
    weights = (expert_gate, expert_up, expert_down)

    far_tokens = swap_halves(moe_tokens)
    far_ids = swap_halves(ids)
    far_route = swap_halves(route)
    last = gate_inner.shape[0] - (conv_taps.shape[0] - 1)
    previous = from_behind(gated_input(gate_inner[last:], conv_input[last:]), EVERY, 1)
    slot, mix, send = to_slots(
        place, ids, route, moe_tokens, gain, slots, capacity, members, WIDE_VMEM
    )
    far_slot, far_mix, far_send = to_slots(
        place, far_ids, far_route, far_tokens, gain, slots, capacity, 1, SMALL_VMEM
    )
    far_received = exchange(far_send[0], members)
    received = in_order(send[0], hops(send, masks))
    far_out = expert_rows([far_received], weights)
    far_back = exchange(far_out[0], members)
    out = expert_rows(received, weights)
    back = hops(out, masks[: members // 2])
    far_total = from_slots(far_slot, far_mix, [far_back], ())
    returned = swap_halves(far_total)
    back |= hops(out, masks[members // 2 :])
    mixed_out = mixer(
        gate_outer, gate_inner, conv_input, previous, conv_taps, mixer_out_weight
    )
    back = in_order(out[0], back)
    moe_out = from_slots(slot, mix, back, (returned,))
    return (mixed_out, moe_out)


def solution(mesh):
    outer, inner = mesh.shape["ep"], mesh.shape["tp"]
    halves = 2 if outer % 2 == 0 else 1
    split = Mesh(mesh.devices.reshape(halves, outer // halves, inner), EVERY)
    rows = P(EVERY, None)
    weights = P(EVERY, None, None)
    in_specs = (rows, rows, rows, P(), P(), rows, P(), rows, rows, weights, weights, weights)
    return jax.shard_map(
        shards, mesh=split, in_specs=in_specs, out_specs=(rows, rows), check_vma=False
    )
```

time: 194 us -> 179 us (0.923)
  blocking collectives: 74.9 us -> 25.5 us
  starting transfers between devices: 7.84 us -> 39.8 us
  Pallas kernels: 0 us -> 27.7 us
  matrix products: 20.5 us -> 8.21 us
  other arithmetic: 12.5 us -> 2.84 us
  local copies, waits for them, and re-layouts: 10.7 us -> 1.41 us
  waiting for transfers between devices: 66 us -> 71.6 us
    ppermute x0 -> x34, waiting for transfers between devices: none -> 71.6 us  [the longest x4 39.7 us: swap_halves(): return lax.ppermute(value, ('half', 'near'), pairs)]
    ppermute x1, waiting for transfers between devices: 66 us -> 0.01 us  [from_behind(): return lax.ppermute(value, axis, pairs)]
    all_to_all x1, blocking collectives: 74.9 us -> 25.5 us  [exchange(): lax.all_to_all(parts, NEAR, split_axis=0, concat_axis=0, tiled=True)]
    ppermute x0 -> x34, starting transfers between devices: none -> 33.8 us  [the longest x30 31.1 us: hops(): lax.ppermute(blocks[mask], NEAR, [(i, i ^ mask) for i in range(members)])]
    pallas_call x0 -> x6, Pallas kernels: none -> 27.7 us  [the longest x2 21.2 us: expert_rows(): pl.pallas_call(functools.partial(expert_kernel, len(rows)), in_specs=[pl....]
    dot_general x5 -> x1, matrix products: 20.5 us -> 8.21 us  [mixer(): jnp.dot(gated_rows, mixer_out_weight, preferred_element_type=jnp.float32)]
    reduce_sum x4 -> x0, other arithmetic: 7.56 us -> none  [the longest x1 6.2 us: shards(): jnp.sum(picked * mix_weight[:, :, None], axis=1).astype(jnp.bfloat16)]
    convert_element_type x1 -> x0, local copies, waits for them, and re-layouts: 4.75 us -> none  [shards(): flat_rows[slot_index.reshape(-1)].astype(jnp.float32)]
  transfers between devices with their start and end apart: 2 -> 36, of which waited for: 1 -> 15; matrix products, arithmetic and copies ran while one was open for 5% -> 6% of each run, Pallas kernels for 0% -> 8%
where the time goes in v2:
time: 179 us; the launch traced here: 178 us
  waiting for transfers between devices  71.6 us (40%)
  starting transfers between devices  39.8 us (22%)
  Pallas kernels  27.7 us (15%)
  blocking collectives  25.5 us (14%)
  matrix products  8.21 us (5%)
  other arithmetic  2.84 us (2%)
    ppermute x4, waiting for transfers between devices, swap_halves(): return lax.ppermute(value, ('half', 'near'), pairs)  39.7 us
    ppermute x30, waiting for transfers between devices, hops(): lax.ppermute(blocks[mask], NEAR, [(i, i ^ mask) for i in range(members)])  31.9 us
    ppermute x30, starting transfers between devices, hops(): lax.ppermute(blocks[mask], NEAR, [(i, i ^ mask) for i in range(members)])  31.1 us
    all_to_all x1, blocking collectives, exchange(): lax.all_to_all(parts, NEAR, split_axis=0, concat_axis=0, tiled=True)  25.5 us
    pallas_call x2, Pallas kernels, expert_rows(): pl.pallas_call(functools.partial(expert_kernel, len(rows)), in_specs=[pl....  21.2 us
    dot_general x1, matrix products, mixer(): jnp.dot(gated_rows, mixer_out_weight, preferred_element_type=jnp.float32)  8.21 us
    pallas_call x2, Pallas kernels, to_slots(): pl.pallas_call(functools.partial(dispatch_kernel, capacity, blocks > 1),...  4.22 us
    all_to_all x1, starting transfers between devices, exchange(): lax.all_to_all(parts, NEAR, split_axis=0, concat_axis=0, tiled=True)  3.85 us
  transfers between devices with their start and end apart: 36, of which 15 were waited for; matrix products, arithmetic and copies ran while one was open for 6% of the time, Pallas kernels for 8%

profile of v2, /device:TPU:16, one launch (start us, length us, event | category | flops | bytes accessed | tf_op | source)
XLA Modules:
  0.0 178.2 jit_solution(6521324510347176995)
XLA Ops:
  3.2 22.7 %collective-permute-done.31.ids_ref = s32[4,128]{1,0:T(4,128)S(1)} collective-permute-done((s32[4,128]{1,0:T(4,128)}, s32[4,128]{1,0:T(4,128)S(1)}, u32[]{:S(2)}, u32[]{:S(2)}) %collective-permute-start.31) | collective-permute-done | bytes 2080 | tf_op jit(solution)/shard_map/ppermute | solution.py:35
  28.0 25.5 %all_to_all.10 = bf16[16,24,2048]{2,1,0:T(8,128)(2,1)} all-to-all(bf16[16,24,2048]{2,1,0:T(8,128)(2,1)S(1)} %bitcast.14), channel_id=1, replica_groups=mesh['half'=2,'near'=4,'tp'=4] {'near','tp'}, dimensions={0} | all-to-all | bytes 3145728 | tf_op jit(solution)/shard_map/all_to_all | solution.py:264
  53.5 10.5 %shard_map.134 = bf16[384,2048]{1,0:T(8,128)(2,1)} custom-call(bf16[1,2048,1024]{2,1,0:T(8,128)(2,1)} %gate.3, bf16[1,2048,1024]{2,1,0:T(8,128)(2,1)} %up.3, bf16[1,1024,2048]{2,1,0:T(8,128)(2,1)} %down.3, bf16[384,2048]{1,0:T(8,128)(2,1)} %bitcast.18), custom_call_target="tpu_custom_call" | custom-call | flops 4831838208 | bytes 15728640 | tf_op jit(solution)/shard_map/pallas_call | solution.py:217
  64.1 3.9 %all-to-all-start.1 = ((bf16[16,24,2048]{2,1,0:T(8,128)(2,1)}), bf16[16,24,2048]{2,1,0:T(8,128)(2,1)S(1)}, u32[]{:S(2)}, u32[]{:S(2)}) async-start(bf16[16,24,2048]{2,1,0:T(8,128)(2,1)} %bitcast.17), calls=%async_computation.1 | async-start | bytes 3145728 | tf_op jit(solution)/shard_map/all_to_all | solution.py:264
  67.9 2.9 %shard_map.131 = (s32[4,128]{1,0:T(4,128)}, f32[4,128]{1,0:T(4,128)}, bf16[24,2048]{1,0:T(8,128)(2,1)}, bf16[24,2048]{1,0:T(8,128)(2,1)}, bf16[24,2048]{1,0:T(8,...) custom-call(s32[2]{0:T(128)} %copy-done.4, ...), custom_call_target="tpu_custom_call" | custom-call | flops 201326592 | bytes 2097152 | tf_op jit(solution)/shard_map/pallas_call | solution.py:92
  71.2 2.6 %collective-permute-start.10 = (bf16[24,2048]{1,0:T(8,128)(2,1)}, bf16[24,2048]{1,0:T(8,128)(2,1)S(1)}, u32[]{:S(2)}, u32[]{:S(2)}) collective-permute-start(bf16[24,2048]{1,0:T(8,128)(2,1)} %get-tuple-element.51), channel_id=1, source_target_pairs={{0,10},{1,11},{2,8},{3,9},{4,14},{5,15},{6,12},{7,13},{8,2},{9,3},... | collective-permute-start | bytes 294920 | tf_op jit(solution)/shard_map/ppermute | solution.py:252
  73.8 2.6 %collective-permute-start.12 = (bf16[24,2048]{1,0:T(8,128)(2,1)}, bf16[24,2048]{1,0:T(8,128)(2,1)S(1)}, u32[]{:S(2)}, u32[]{:S(2)}) collective-permute-start(bf16[24,2048]{1,0:T(8,128)(2,1)} %get-tuple-element.53), channel_id=1, source_target_pairs={{0,12},{1,13},{2,14},{3,15},{4,8},{5,9},{6,10},{7,11},{8,4},{9,5},... | collective-permute-start | bytes 294920 | tf_op jit(solution)/shard_map/ppermute | solution.py:252
  76.5 3.5 %collective-permute-start.14 = (bf16[24,2048]{1,0:T(8,128)(2,1)}, bf16[24,2048]{1,0:T(8,128)(2,1)S(1)}, u32[]{:S(2)}, u32[]{:S(2)}) collective-permute-start(bf16[24,2048]{1,0:T(8,128)(2,1)} %get-tuple-element.55), channel_id=1, source_target_pairs={{0,14},{1,15},{2,12},{3,13},{4,10},{5,11},{6,8},{7,9},{8,6},{9,7},... | collective-permute-start | bytes 294920 | tf_op jit(solution)/shard_map/ppermute | solution.py:252
  80.0 12.6 %collective-permute-done.10.refs_10_ = bf16[24,2048]{1,0:T(8,128)(2,1)S(1)} collective-permute-done((bf16[24,2048]{1,0:T(8,128)(2,1)}, bf16[24,2048]{1,0:T(8,128)(2,1)S(1)}, u32[]{:S(2)}, u32[]{:S(2)}) %collective-permute-start.10) | collective-permute-done | bytes 98336 | tf_op jit(solution)/shard_map/ppermute | solution.py:252
  93.6 3.3 %collective-permute-done.12.refs_12_ = bf16[24,2048]{1,0:T(8,128)(2,1)S(1)} collective-permute-done((bf16[24,2048]{1,0:T(8,128)(2,1)}, bf16[24,2048]{1,0:T(8,128)(2,1)S(1)}, u32[]{:S(2)}, u32[]{:S(2)}) %collective-permute-start.12) | collective-permute-done | bytes 98336 | tf_op jit(solution)/shard_map/ppermute | solution.py:252
  97.9 3.7 %collective-permute-done.14.refs_14_ = bf16[24,2048]{1,0:T(8,128)(2,1)S(1)} collective-permute-done((bf16[24,2048]{1,0:T(8,128)(2,1)}, bf16[24,2048]{1,0:T(8,128)(2,1)S(1)}, u32[]{:S(2)}, u32[]{:S(2)}) %collective-permute-start.14) | collective-permute-done | bytes 98336 | tf_op jit(solution)/shard_map/ppermute | solution.py:252
  103.6 1.7 collective-permute-start.7
  107.9 3.7 %collective-permute-done.5.refs_5_ = bf16[24,2048]{1,0:T(8,128)(2,1)S(1)} collective-permute-done((bf16[24,2048]{1,0:T(8,128)(2,1)}, bf16[24,2048]{1,0:T(8,128)(2,1)S(1)}, u32[]{:S(2)}, u32[]{:S(2)}) %collective-permute-start.5) | collective-permute-done | bytes 98336 | tf_op jit(solution)/shard_map/ppermute | solution.py:252
  111.6 2.2 %collective-permute-start = (bf16[2,1024]{1,0:T(2,128)(2,1)S(1)}, bf16[2,1024]{1,0:T(2,128)(2,1)S(1)}, u32[]{:S(2)}, u32[]{:S(2)}) collective-permute-start(bf16[2,1024]{1,0:T(2,128)(2,1)S(1)} %multiply_convert_fusion.1), channel_id=1, source_target_pairs={{0,1},{1,2},{2,3},{3,4},{4,5},{5,6},{6,7},{7,8},{8,9},{9,10},{10,1... | collective-permute-start | bytes 12296 | tf_op jit(solution)/shard_map/ppermute | solution.py:24
  114.5 10.6 %shard_map.132 = (bf16[24,2048]{1,0:T(8,128)(2,1)}, bf16[24,2048]{1,0:T(8,128)(2,1)}, bf16[24,2048]{1,0:T(8,128)(2,1)}, bf16[24,2048]{1,0:T(8,128)(2,1)}, bf16[2...) custom-call(bf16[1,2048,1024]{2,1,0:T(8,128)(2,1)} %gate.3, ...), custom_call_target="tpu_custom_call" | custom-call | flops 4831838208 | bytes 15728640 | tf_op jit(solution)/shard_map/pallas_call | solution.py:217
  130.4 1.7 collective-permute-start.21
  134.2 1.7 collective-permute-start.24
  135.9 3.7 %collective-permute-done.20.refs_5_ = bf16[24,2048]{1,0:T(8,128)(2,1)S(1)} collective-permute-done((bf16[24,2048]{1,0:T(8,128)(2,1)S(1)}, bf16[24,2048]{1,0:T(8,128)(2,1)S(1)}, u32[]{:S(2)}, u32[]{:S(2)}) %collective-permute-start.20) | collective-permute-done | bytes 98336 | tf_op jit(solution)/shard_map/ppermute | solution.py:252
  140.4 2.2 %collective-permute-start.26 = (bf16[24,2048]{1,0:T(8,128)(2,1)S(1)}, bf16[24,2048]{1,0:T(8,128)(2,1)S(1)}, u32[]{:S(2)}, u32[]{:S(2)}) collective-permute-start(bf16[24,2048]{1,0:T(8,128)(2,1)S(1)} %copy-done.13), channel_id=1, source_target_pairs={{0,11},{1,10},{2,9},{3,8},{4,15},{5,14},{6,13},{7,12},{8,3},{9,2},... | collective-permute-start | bytes 294920 | tf_op jit(solution)/shard_map/ppermute | solution.py:252
  142.5 1.6 maximum_convert_fusion
  145.6 1.9 %collective-permute-start.28 = (bf16[24,2048]{1,0:T(8,128)(2,1)S(1)}, bf16[24,2048]{1,0:T(8,128)(2,1)S(1)}, u32[]{:S(2)}, u32[]{:S(2)}) collective-permute-start(bf16[24,2048]{1,0:T(8,128)(2,1)S(1)} %copy-done.11), channel_id=1, source_target_pairs={{0,13},{1,12},{2,15},{3,14},{4,9},{5,8},{6,11},{7,10},{8,5},{9,4},... | collective-permute-start | bytes 294920 | tf_op jit(solution)/shard_map/ppermute | solution.py:252
  148.8 2.5 %collective-permute-start.30 = (bf16[24,2048]{1,0:T(8,128)(2,1)S(1)}, bf16[24,2048]{1,0:T(8,128)(2,1)S(1)}, u32[]{:S(2)}, u32[]{:S(2)}) collective-permute-start(bf16[24,2048]{1,0:T(8,128)(2,1)S(1)} %copy-done.9), channel_id=1, source_target_pairs={{0,15},{1,14},{2,13},{3,12},{4,11},{5,10},{6,9},{7,8},{8,7},{9,6},... | collective-permute-start | bytes 294920 | tf_op jit(solution)/shard_map/ppermute | solution.py:252
  151.4 8.2 %convolution_convert_fusion = bf16[512,2048]{1,0:T(8,128)(2,1)} fusion(bf16[1024,2048]{1,0:T(8,128)(2,1)} %param.16, f32[514,1024]{1,0:T(8,128)} %maximum_convert_fusion, bf16[512,1024]{1,0:T(8,128)(2,1)S(1)} %copy-done.8, f32[1024]{0:T(1024)S(1)} %bitcast.20, f32[1024]{0:T(1024)S(1)} %bitcast.21, f32[1024]{0:T(1024)S(1)} %bitcast.19), kind=kOutput, calls=%fused_computation | convolution fusion | flops 2152726528 | bytes 13643776 | tf_op jit(solution)/shard_map/dot_general | solution.py:279
  159.6 17.0 %collective-permute-done.34.refs_16_ = bf16[128,2048]{1,0:T(8,128)(2,1)S(1)} collective-permute-done((bf16[128,2048]{1,0:T(8,128)(2,1)S(1)}, bf16[128,2048]{1,0:T(8,128)(2,1)S(1)}, u32[]{:S(2)}, u32[]{:S(2)}) %collective-permute-start.34) | collective-permute-done | bytes 524320 | tf_op jit(solution)/shard_map/ppermute | solution.py:35
  (135 shorter events, 24.5 us)
Async XLA Ops:
  0.6 25.4 %collective-permute-start.33 = (bf16[128,2048]{1,0:T(8,128)(2,1)}, bf16[128,2048]{1,0:T(8,128)(2,1)S(1)}, u32[]{:S(2)}, u32[]{:S(2)}) collective-permute-start(bf16[128,2048]{1,0:T(8,128)(2,1)} %rows_ref.1), channel_id=1, source_target_pairs={{0,24},{4,28},{8,16},{12,20},{16,8},{20,12},{24,0},{28,4},{1,25},{... | collective-permute-start | bytes 1572872 | tf_op jit(solution)/shard_map/ppermute | solution.py:35
  1.1 24.8 %collective-permute-start.31 = (s32[4,128]{1,0:T(4,128)}, s32[4,128]{1,0:T(4,128)S(1)}, u32[]{:S(2)}, u32[]{:S(2)}) collective-permute-start(s32[4,128]{1,0:T(4,128)} %bitcast.22), channel_id=1, source_target_pairs={{0,24},{4,28},{8,16},{12,20},{16,8},{20,12},{24,0},{28,4},{1,25},{... | collective-permute-start | bytes 6152 | tf_op jit(solution)/shard_map/ppermute | solution.py:35
  2.7 23.3 %collective-permute-start.32 = (f32[4,128]{1,0:T(4,128)}, f32[4,128]{1,0:T(4,128)S(1)}, u32[]{:S(2)}, u32[]{:S(2)}) collective-permute-start(f32[4,128]{1,0:T(4,128)} %bitcast.24), channel_id=1, source_target_pairs={{0,24},{4,28},{8,16},{12,20},{16,8},{20,12},{24,0},{28,4},{1,25},{... | collective-permute-start | bytes 6152 | tf_op jit(solution)/shard_map/ppermute | solution.py:35
  64.1 80.1 %all-to-all-start.1 = ((bf16[16,24,2048]{2,1,0:T(8,128)(2,1)}), bf16[16,24,2048]{2,1,0:T(8,128)(2,1)S(1)}, u32[]{:S(2)}, u32[]{:S(2)}) async-start(bf16[16,24,2048]{2,1,0:T(8,128)(2,1)} %bitcast.17), calls=%async_computation.1 | async-start | bytes 3145728 | tf_op jit(solution)/shard_map/all_to_all | solution.py:264
  71.2 21.4 %collective-permute-start.10 = (bf16[24,2048]{1,0:T(8,128)(2,1)}, bf16[24,2048]{1,0:T(8,128)(2,1)S(1)}, u32[]{:S(2)}, u32[]{:S(2)}) collective-permute-start(bf16[24,2048]{1,0:T(8,128)(2,1)} %get-tuple-element.51), channel_id=1, source_target_pairs={{0,10},{1,11},{2,8},{3,9},{4,14},{5,15},{6,12},{7,13},{8,2},{9,3},... | collective-permute-start | bytes 294920 | tf_op jit(solution)/shard_map/ppermute | solution.py:252
  73.8 19.8 %collective-permute-start.11 = (bf16[24,2048]{1,0:T(8,128)(2,1)}, bf16[24,2048]{1,0:T(8,128)(2,1)S(1)}, u32[]{:S(2)}, u32[]{:S(2)}) collective-permute-start(bf16[24,2048]{1,0:T(8,128)(2,1)} %get-tuple-element.52), channel_id=1, source_target_pairs={{0,11},{1,10},{2,9},{3,8},{4,15},{5,14},{6,13},{7,12},{8,3},{9,2},... | collective-permute-start | bytes 294920 | tf_op jit(solution)/shard_map/ppermute | solution.py:252
  73.8 23.2 %collective-permute-start.12 = (bf16[24,2048]{1,0:T(8,128)(2,1)}, bf16[24,2048]{1,0:T(8,128)(2,1)S(1)}, u32[]{:S(2)}, u32[]{:S(2)}) collective-permute-start(bf16[24,2048]{1,0:T(8,128)(2,1)} %get-tuple-element.53), channel_id=1, source_target_pairs={{0,12},{1,13},{2,14},{3,15},{4,8},{5,9},{6,10},{7,11},{8,4},{9,5},... | collective-permute-start | bytes 294920 | tf_op jit(solution)/shard_map/ppermute | solution.py:252
  76.4 21.5 %collective-permute-start.13 = (bf16[24,2048]{1,0:T(8,128)(2,1)}, bf16[24,2048]{1,0:T(8,128)(2,1)S(1)}, u32[]{:S(2)}, u32[]{:S(2)}) collective-permute-start(bf16[24,2048]{1,0:T(8,128)(2,1)} %get-tuple-element.54), channel_id=1, source_target_pairs={{0,13},{1,12},{2,15},{3,14},{4,9},{5,8},{6,11},{7,10},{8,5},{9,4},... | collective-permute-start | bytes 294920 | tf_op jit(solution)/shard_map/ppermute | solution.py:252
  76.5 25.1 %collective-permute-start.14 = (bf16[24,2048]{1,0:T(8,128)(2,1)}, bf16[24,2048]{1,0:T(8,128)(2,1)S(1)}, u32[]{:S(2)}, u32[]{:S(2)}) collective-permute-start(bf16[24,2048]{1,0:T(8,128)(2,1)} %get-tuple-element.55), channel_id=1, source_target_pairs={{0,14},{1,15},{2,12},{3,13},{4,10},{5,11},{6,8},{7,9},{8,6},{9,7},... | collective-permute-start | bytes 294920 | tf_op jit(solution)/shard_map/ppermute | solution.py:252
  92.6 10.1 %collective-permute-start.15 = (bf16[24,2048]{1,0:T(8,128)(2,1)}, bf16[24,2048]{1,0:T(8,128)(2,1)S(1)}, u32[]{:S(2)}, u32[]{:S(2)}) collective-permute-start(bf16[24,2048]{1,0:T(8,128)(2,1)} %get-tuple-element.56), channel_id=1, source_target_pairs={{0,15},{1,14},{2,13},{3,12},{4,11},{5,10},{6,9},{7,8},{8,7},{9,6},... | collective-permute-start | bytes 294920 | tf_op jit(solution)/shard_map/ppermute | solution.py:252
  93.5 10.1 %collective-permute-start.2 = (bf16[24,2048]{1,0:T(8,128)(2,1)}, bf16[24,2048]{1,0:T(8,128)(2,1)S(1)}, u32[]{:S(2)}, u32[]{:S(2)}) collective-permute-start(bf16[24,2048]{1,0:T(8,128)(2,1)} %get-tuple-element.43), channel_id=1, source_target_pairs={{0,2},{1,3},{2,0},{3,1},{4,6},{5,7},{6,4},{7,5},{8,10},{9,11},{10,... | collective-permute-start | bytes 294920 | tf_op jit(solution)/shard_map/ppermute | solution.py:252
  102.7 11.1 %collective-permute-start.6 = (bf16[24,2048]{1,0:T(8,128)(2,1)}, bf16[24,2048]{1,0:T(8,128)(2,1)S(1)}, u32[]{:S(2)}, u32[]{:S(2)}) collective-permute-start(bf16[24,2048]{1,0:T(8,128)(2,1)} %get-tuple-element.47), channel_id=1, source_target_pairs={{0,6},{1,7},{2,4},{3,5},{4,2},{5,3},{6,0},{7,1},{8,14},{9,15},{10,... | collective-permute-start | bytes 294920 | tf_op jit(solution)/shard_map/ppermute | solution.py:252
  103.6 10.2 %collective-permute-start.7 = (bf16[24,2048]{1,0:T(8,128)(2,1)}, bf16[24,2048]{1,0:T(8,128)(2,1)S(1)}, u32[]{:S(2)}, u32[]{:S(2)}) collective-permute-start(bf16[24,2048]{1,0:T(8,128)(2,1)} %get-tuple-element.48), channel_id=1, source_target_pairs={{0,7},{1,6},{2,5},{3,4},{4,3},{5,2},{6,1},{7,0},{8,15},{9,14},{10,... | collective-permute-start | bytes 294920 | tf_op jit(solution)/shard_map/ppermute | solution.py:252
  111.6 17.7 %collective-permute-start = (bf16[2,1024]{1,0:T(2,128)(2,1)S(1)}, bf16[2,1024]{1,0:T(2,128)(2,1)S(1)}, u32[]{:S(2)}, u32[]{:S(2)}) collective-permute-start(bf16[2,1024]{1,0:T(2,128)(2,1)S(1)} %multiply_convert_fusion.1), channel_id=1, source_target_pairs={{0,1},{1,2},{2,3},{3,4},{4,5},{5,6},{6,7},{7,8},{8,9},{9,10},{10,1... | collective-permute-start | bytes 12296 | tf_op jit(solution)/shard_map/ppermute | solution.py:24
  129.3 10.4 %collective-permute-start.20 = (bf16[24,2048]{1,0:T(8,128)(2,1)S(1)}, bf16[24,2048]{1,0:T(8,128)(2,1)S(1)}, u32[]{:S(2)}, u32[]{:S(2)}) collective-permute-start(bf16[24,2048]{1,0:T(8,128)(2,1)S(1)} %copy-done.28), channel_id=1, source_target_pairs={{0,5},{1,4},{2,7},{3,6},{4,1},{5,0},{6,3},{7,2},{8,13},{9,12},{10,... | collective-permute-start | bytes 294920 | tf_op jit(solution)/shard_map/ppermute | solution.py:252
  132.5 12.4 %collective-permute-start.22 = (bf16[24,2048]{1,0:T(8,128)(2,1)}, bf16[24,2048]{1,0:T(8,128)(2,1)S(1)}, u32[]{:S(2)}, u32[]{:S(2)}) collective-permute-start(bf16[24,2048]{1,0:T(8,128)(2,1)} %get-tuple-element.64), channel_id=1, source_target_pairs={{0,7},{1,6},{2,5},{3,4},{4,3},{5,2},{6,1},{7,0},{8,15},{9,14},{10,... | collective-permute-start | bytes 294920 | tf_op jit(solution)/shard_map/ppermute | solution.py:252
  133.3 12.4 %collective-permute-start.23 = (bf16[24,2048]{1,0:T(8,128)(2,1)S(1)}, bf16[24,2048]{1,0:T(8,128)(2,1)S(1)}, u32[]{:S(2)}, u32[]{:S(2)}) collective-permute-start(bf16[24,2048]{1,0:T(8,128)(2,1)S(1)} %copy-done.21), channel_id=1, source_target_pairs={{0,8},{1,9},{2,10},{3,11},{4,12},{5,13},{6,14},{7,15},{8,0},{9,1},... | collective-permute-start | bytes 294920 | tf_op jit(solution)/shard_map/ppermute | solution.py:252
  134.2 13.4 %collective-permute-start.24 = (bf16[24,2048]{1,0:T(8,128)(2,1)S(1)}, bf16[24,2048]{1,0:T(8,128)(2,1)S(1)}, u32[]{:S(2)}, u32[]{:S(2)}) collective-permute-start(bf16[24,2048]{1,0:T(8,128)(2,1)S(1)} %copy-done.19), channel_id=1, source_target_pairs={{0,9},{1,8},{2,11},{3,10},{4,13},{5,12},{6,15},{7,14},{8,1},{9,0},... | collective-permute-start | bytes 294920 | tf_op jit(solution)/shard_map/ppermute | solution.py:252
  140.4 10.9 %collective-permute-start.26 = (bf16[24,2048]{1,0:T(8,128)(2,1)S(1)}, bf16[24,2048]{1,0:T(8,128)(2,1)S(1)}, u32[]{:S(2)}, u32[]{:S(2)}) collective-permute-start(bf16[24,2048]{1,0:T(8,128)(2,1)S(1)} %copy-done.13), channel_id=1, source_target_pairs={{0,11},{1,10},{2,9},{3,8},{4,15},{5,14},{6,13},{7,12},{8,3},{9,2},... | collective-permute-start | bytes 294920 | tf_op jit(solution)/shard_map/ppermute | solution.py:252
  145.0 14.6 %collective-permute-start.27 = (bf16[24,2048]{1,0:T(8,128)(2,1)S(1)}, bf16[24,2048]{1,0:T(8,128)(2,1)S(1)}, u32[]{:S(2)}, u32[]{:S(2)}) collective-permute-start(bf16[24,2048]{1,0:T(8,128)(2,1)S(1)} %copy-done.12), channel_id=1, source_target_pairs={{0,12},{1,13},{2,14},{3,15},{4,8},{5,9},{6,10},{7,11},{8,4},{9,5},... | collective-permute-start | bytes 294920 | tf_op jit(solution)/shard_map/ppermute | solution.py:252
  145.6 14.0 %collective-permute-start.28 = (bf16[24,2048]{1,0:T(8,128)(2,1)S(1)}, bf16[24,2048]{1,0:T(8,128)(2,1)S(1)}, u32[]{:S(2)}, u32[]{:S(2)}) collective-permute-start(bf16[24,2048]{1,0:T(8,128)(2,1)S(1)} %copy-done.11), channel_id=1, source_target_pairs={{0,13},{1,12},{2,15},{3,14},{4,9},{5,8},{6,11},{7,10},{8,5},{9,4},... | collective-permute-start | bytes 294920 | tf_op jit(solution)/shard_map/ppermute | solution.py:252
  147.6 12.0 %collective-permute-start.29 = (bf16[24,2048]{1,0:T(8,128)(2,1)S(1)}, bf16[24,2048]{1,0:T(8,128)(2,1)S(1)}, u32[]{:S(2)}, u32[]{:S(2)}) collective-permute-start(bf16[24,2048]{1,0:T(8,128)(2,1)S(1)} %copy-done.10), channel_id=1, source_target_pairs={{0,14},{1,15},{2,12},{3,13},{4,10},{5,11},{6,8},{7,9},{8,6},{9,7},... | collective-permute-start | bytes 294920 | tf_op jit(solution)/shard_map/ppermute | solution.py:252
  148.8 10.8 %collective-permute-start.30 = (bf16[24,2048]{1,0:T(8,128)(2,1)S(1)}, bf16[24,2048]{1,0:T(8,128)(2,1)S(1)}, u32[]{:S(2)}, u32[]{:S(2)}) collective-permute-start(bf16[24,2048]{1,0:T(8,128)(2,1)S(1)} %copy-done.9), channel_id=1, source_target_pairs={{0,15},{1,14},{2,13},{3,12},{4,11},{5,10},{6,9},{7,8},{8,7},{9,6},... | collective-permute-start | bytes 294920 | tf_op jit(solution)/shard_map/ppermute | solution.py:252
  151.3 25.3 %collective-permute-start.34 = (bf16[128,2048]{1,0:T(8,128)(2,1)S(1)}, bf16[128,2048]{1,0:T(8,128)(2,1)S(1)}, u32[]{:S(2)}, u32[]{:S(2)}) collective-permute-start(bf16[128,2048]{1,0:T(8,128)(2,1)S(1)} %shard_map.135), channel_id=1, source_target_pairs={{0,24},{4,28},{8,16},{12,20},{16,8},{20,12},{24,0},{28,4},{1,25},{... | collective-permute-start | bytes 1572872 | tf_op jit(solution)/shard_map/ppermute | solution.py:35
  (49 other events, 551.5 us)
